TPU v7x, 256 devices: a 8x8x2 block of a 8x8x16 slice. The times are simulated.
256 devices in a mesh: grp: 2 (over z), ep: 16 (over y, core), tp: 8 (over x).
Axes of the slice: x: 8, y: 8, z: 2, core: 2. Of those that a mesh axis runs over, the one named last changes fastest.
The devices are a block of a 8x8x16 slice.
Arguments:
- tokens: bfloat16 [8192, 4096], P(('grp', 'ep')), parts along dimension 0, may hold values from -6 to 6
- expert_ids: int32 [8192, 2], P(('grp', 'ep')), parts along dimension 0, may hold values from 0 to 15, as said below
- gates: float32 [8192, 2], P(('grp', 'ep')), parts along dimension 0, may hold values from 0.1 to 1
- w_gate: bfloat16 [16, 4096, 2048], P('ep', None, 'tp'), may hold values from -0.09375 to 0.09375
- w_up: bfloat16 [16, 4096, 2048], P('ep', None, 'tp'), may hold values from -0.09375 to 0.09375
- w_down: bfloat16 [16, 2048, 4096], P('ep', 'tp'), may hold values from -0.79549513 to 0.79549513, as said below
- norm_gain: float32 [4096], P('tp'), may hold values from 0.1 to 1.9
- norm_bias: float32 [4096], P('tp'), may hold values from -1.5 to 1.5
Outputs:
- normed: bfloat16 [8192, 4096], P(('grp', 'ep'), 'tp'), parts along dimension 0
There are 2 independent parts, one for each index of `grp`. A program takes and returns all parts, laid end to end along the dimension named above; an argument that names none is the same for every part. Nothing has to cross between parts.
Inputs may be any that keep to these rules, and one draw needn't show every extreme that they name: `expert_ids`: each row names 2 different experts, both in the same group of 4 consecutive expert numbers. Within one aligned block of 256 rows no expert is named more than 64 times, and in every draw some expert is named exactly 64 times in every block. `w_down`: down projection weights.
All inputs are finite; a program needn't handle non-finite values.
Results may differ from a plain program's by a relative error of at most 0.014.
Values may be sent and summed in bfloat16 or wider, within the bound.
No kernel may reach another device: no remote copies, remote signals or barrier semaphores. Data moves between devices by JAX's collectives and lax.ppermute only.
A program may use at most 128 MiB of HBM per device.

v0:
```python
import jax
import jax.numpy as jnp
from jax import lax
from jax.sharding import PartitionSpec as P

D = 4096
EXPERTS = 16
CAP = 64
RING_PARTS = 3
ALL_PARTS = 4

norm_eps = 1e-05


def f32_dot(a, b, dims=(((1,), (0,)), ((), ()))):
    return lax.dot_general(a, b, dims, preferred_element_type=jnp.float32)


def route(expert_ids, gates):
    ids = expert_ids.T
    tok = ids.shape[1]
    experts = jnp.arange(EXPERTS, dtype=jnp.int32)[:, None]
    first = ids[0][None, :] == experts
    second = ids[1][None, :] == experts
    named = jnp.logical_or(first, second).astype(jnp.bfloat16)
    row = jnp.arange(tok, dtype=jnp.int32)
    before = (row[:, None] < row[None, :]).astype(jnp.bfloat16)
    slot = f32_dot(named, before).astype(jnp.int32) + experts * CAP
    target0 = jnp.sum(jnp.where(first, slot, 0), axis=0)
    target1 = jnp.sum(jnp.where(second, slot, 0), axis=0)
    slots = jnp.arange(EXPERTS * CAP, dtype=jnp.int32)[:, None]
    at0 = slots == target0[None, :]
    at1 = slots == target1[None, :]
    send = jnp.logical_or(at0, at1).astype(jnp.bfloat16)
    g = gates.T
    weight = jnp.where(at0, g[0][None, :], 0.0) + jnp.where(at1, g[1][None, :], 0.0)
    high = lax.reduce_precision(weight, 8, 7)
    return send, high.astype(jnp.bfloat16), (weight - high).astype(jnp.bfloat16)


def layer(tokens, expert_ids, gates, w_gate, w_up, w_down, norm_gain, norm_bias):
    tok_rows, _ = tokens.shape
    n_tp = lax.axis_size("tp")
    n_ep = lax.axis_size("ep")
    me = lax.axis_index("tp")
    piece = norm_gain.shape[0]
    ring_piece = piece * RING_PARTS // ALL_PARTS
    flat_piece = piece - ring_piece
    ring_width = ring_piece * n_tp
    flat_width = flat_piece * n_tp
    right = [(i, (i + 1) % n_tp) for i in range(n_tp)]
    left = [(i, (i - 1) % n_tp) for i in range(n_tp)]
    far = n_tp // 2

    def at(i):
        return lax.rem(me + i + n_tp, n_tp)

    wd = w_down[0]
    rows = n_ep * CAP
    half = rows // 2
    hidden_width = w_up.shape[2]
    send, weight_high, weight_low = route(expert_ids, gates)
    own = lax.dynamic_slice_in_dim(tokens, me * ring_piece, ring_piece, 1)
    out1 = f32_dot(send, own).astype(jnp.bfloat16).reshape(n_ep, CAP, ring_piece)
    out2 = f32_dot(send, tokens[:, ring_width:]).astype(jnp.bfloat16).reshape(n_ep, CAP, flat_width)
    got1 = lax.all_to_all(out1, "ep", 0, 0, tiled=True).reshape(rows, ring_piece)
    w_both = jnp.concatenate([w_gate[0], w_up[0]], axis=1)
    wd2 = wd.reshape(hidden_width, n_tp, piece)[:, :, ring_piece:].reshape(hidden_width, flat_width)
    got1, out2, w_both, wd2, weight_high, weight_low = lax.optimization_barrier(
        (got1, out2, w_both, wd2, weight_high, weight_low)
    )
    got2 = lax.all_to_all(out2, "ep", 0, 0, tiled=True).reshape(rows, flat_width)

    def gate_up(x, start, size):
        return f32_dot(x, lax.dynamic_slice_in_dim(w_both, start, size, 0))

    to_right = got1
    to_left = got1
    for s in range(1, far):
        to_right = lax.ppermute(to_right, "tp", right)
        to_left = lax.ppermute(to_left, "tp", left)
        if s == 1:
            got1, to_right, to_left = lax.optimization_barrier((got1, to_right, to_left))
            acc = gate_up(got1, me * ring_piece, ring_piece)
        acc = acc + gate_up(to_right, at(-s) * ring_piece, ring_piece)
        acc = acc + gate_up(to_left, at(s) * ring_piece, ring_piece)
    far_top = lax.ppermute(to_right[:half], "tp", right)
    far_bottom = lax.ppermute(to_left[half:], "tp", left)
    acc = acc + gate_up(got2, ring_width, flat_width)
    acc = acc + gate_up(jnp.concatenate([far_top, far_bottom], axis=0), at(far) * ring_piece, ring_piece)
    g = acc[:, :hidden_width]
    u = acc[:, hidden_width:]
    hidden = (g / (1.0 + jnp.exp(-g)) * u).astype(jnp.bfloat16)

    def down(x, target):
        return f32_dot(x, lax.dynamic_slice_in_dim(wd, target * piece, ring_piece, 1))

    farthest = down(hidden, at(far)).astype(jnp.bfloat16)
    to_right = lax.ppermute(farthest[:half], "tp", right)
    to_left = lax.ppermute(farthest[half:], "tp", left)
    back2 = f32_dot(hidden, wd2).astype(jnp.bfloat16)
    home2 = lax.all_to_all(back2.reshape(n_ep, CAP, flat_width), "ep", 0, 0, tiled=True).reshape(rows, flat_width)
    seen_right = [to_right]
    seen_left = [to_left]
    for j in range(1, far + 1):
        s = far - j
        tie = max(j - 2, 0)
        x, seen_right[tie], seen_left[tie] = lax.optimization_barrier((hidden, seen_right[tie], seen_left[tie]))
        from_left = seen_right[-1].astype(jnp.float32)
        from_right = seen_left[-1].astype(jnp.float32)
        if j == 1:
            from_left = jnp.pad(from_left, ((0, half), (0, 0)))
            from_right = jnp.pad(from_right, ((half, 0), (0, 0)))
        if s == 0:
            back1 = (down(x, me) + from_left + from_right).astype(jnp.bfloat16)
            break
        to_right = (down(x, at(s)) + from_left).astype(jnp.bfloat16)
        to_left = (down(x, at(-s)) + from_right).astype(jnp.bfloat16)
        seen_right.append(lax.ppermute(to_right, "tp", right))
        seen_left.append(lax.ppermute(to_left, "tp", left))

    first_dims = (((0,), (0,)), ((), ()))

    def combine(x):
        return f32_dot(weight_high, x, first_dims) + f32_dot(weight_low, x, first_dims)

    mixed2 = combine(home2).astype(jnp.bfloat16).reshape(tok_rows, n_tp, flat_piece)
    mixed2 = lax.all_to_all(mixed2.transpose(1, 0, 2), "tp", 0, 0, tiled=True)
    back1, mixed2 = lax.optimization_barrier((back1, mixed2))
    home1 = lax.all_to_all(back1.reshape(n_ep, CAP, ring_piece), "ep", 0, 0, tiled=True).reshape(rows, ring_piece)
    combined = jnp.concatenate([combine(home1), jnp.sum(mixed2.astype(jnp.float32), axis=0)], axis=1)

    stats = jnp.stack([jnp.sum(combined, axis=1), jnp.sum(combined * combined, axis=1)])
    stats = lax.all_to_all(jnp.broadcast_to(stats[None], (n_tp, *stats.shape)), "tp", 0, 0, tiled=True)
    stats = jnp.sum(stats, axis=0)
    row_mean = stats[0] / D
    row_var = stats[1] / D - row_mean * row_mean
    normed = (combined - row_mean[:, None]) * lax.rsqrt(
        row_var[:, None] + norm_eps
    ) * norm_gain + norm_bias
    return normed.astype(jnp.bfloat16)


def solution(mesh):
    return jax.shard_map(
        layer,
        mesh=mesh,
        in_specs=(
            P(("grp", "ep"), None),
            P(("grp", "ep"), None),
            P(("grp", "ep"), None),
            P("ep", None, "tp"),
            P("ep", None, "tp"),
            P("ep", "tp", None),
            P("tp"),
            P("tp"),
        ),
        out_specs=P(("grp", "ep"), "tp"),
        check_vma=False,
    )
```

profile of v0, /device:TPU:513, one launch (start us, length us, event | category | flops | bytes accessed | tf_op | source)
XLA Modules:
  0.0 287.1 jit_solution(17984402656326338544)
XLA Ops:
  0.0 0.9 fusion.84
  1.0 2.3 convolution_convert_fusion.3
  3.3 24.4 %all-to-all-start = ((bf16[16,64,384]{2,1,0:T(8,128)(2,1)}), bf16[16,64,384]{2,1,0:T(8,128)(2,1)}, u32[]{:S(2)}, u32[]{:S(2)}) async-start(bf16[16,64,384]{2,1,0:T(8,128)(2,1)} %bitcast.3), calls=%async_computation | async-start | bytes 1572864 | tf_op jit(solution)/shard_map/all_to_all | solution.py:66
  27.7 0.9 copy.17
  28.9 0.5 copy-done.13
  29.3 1.2 fusion.3
  30.5 3.1 %convolution_convert_fusion.1 = bf16[1024,1024]{1,0:T(8,128)(2,1)} fusion(bf16[256,4096]{1,0:T(8,128)(2,1)} %param.8, s32[256]{0:T(256)S(1)} %get-tuple-element.42, s32[256]{0:T(256)S(1)} %get-tuple-element.41), kind=kOutput, calls=%fused_computation.3 | convolution fusion | flops 538705920 | bytes 2623488 | tf_op jit(solution)/shard_map/dot_general | solution.py:16
  33.6 2.3 pad_maximum_fusion
  35.9 14.7 %all-to-all-done = bf16[16,64,384]{2,1,0:T(8,128)(2,1)} async-done(((bf16[16,64,384]{2,1,0:T(8,128)(2,1)}), bf16[16,64,384]{2,1,0:T(8,128)(2,1)}, u32[]{:S(2)}, u32[]{:S(2)}) %all-to-all-start) | async-done | bytes 786464 | tf_op jit(solution)/shard_map/all_to_all | solution.py:66
  50.6 4.5 %all-to-all-start.1 = ((bf16[16,64,1024]{2,1,0:T(8,128)(2,1)}), bf16[16,64,1024]{2,1,0:T(8,128)(2,1)}, u32[]{:S(2)}, u32[]{:S(2)}) async-start(bf16[16,64,1024]{2,1,0:T(8,128)(2,1)} %bitcast.5), calls=%async_computation.1 | async-start | bytes 4194304 | tf_op jit(solution)/shard_map/all_to_all | solution.py:72
  55.3 2.6 collective-permute-start.1
  57.9 17.9 %collective-permute-done = bf16[1024,384]{1,0:T(8,128)(2,1)} collective-permute-done((bf16[1024,384]{1,0:T(8,128)(2,1)}, bf16[1024,384]{1,0:T(8,128)(2,1)}, u32[]{:S(2)}, u32[]{:S(2)}) %collective-permute-start) | collective-permute-done | bytes 786464 | tf_op jit(solution)/shard_map/ppermute | solution.py:80
  75.8 3.0 %collective-permute-start.3 = (bf16[1024,384]{1,0:T(8,128)(2,1)}, bf16[1024,384]{1,0:T(8,128)(2,1)}, u32[]{:S(2)}, u32[]{:S(2)}) collective-permute-start(bf16[1024,384]{1,0:T(8,128)(2,1)} %collective-permute-done.1), channel_id=1, source_target_pairs={{0,7},{1,0},{2,1},{3,2},{4,3},{5,4},{6,5},{7,6},{8,15},{9,8},{10,9... | collective-permute-start | bytes 2359304 | tf_op jit(solution)/shard_map/ppermute | solution.py:81
  78.7 1.9 fusion.30
  80.7 15.2 %collective-permute-done.3 = bf16[1024,384]{1,0:T(8,128)(2,1)} collective-permute-done((bf16[1024,384]{1,0:T(8,128)(2,1)}, bf16[1024,384]{1,0:T(8,128)(2,1)}, u32[]{:S(2)}, u32[]{:S(2)}) %collective-permute-start.3) | collective-permute-done | bytes 786464 | tf_op jit(solution)/shard_map/ppermute | solution.py:81
  95.8 3.4 %collective-permute-start.5 = (bf16[1024,384]{1,0:T(8,128)(2,1)}, bf16[1024,384]{1,0:T(8,128)(2,1)S(1)}, u32[]{:S(2)}, u32[]{:S(2)}) collective-permute-start(bf16[1024,384]{1,0:T(8,128)(2,1)} %collective-permute-done.3), channel_id=1, source_target_pairs={{0,7},{1,0},{2,1},{3,2},{4,3},{5,4},{6,5},{7,6},{8,15},{9,8},{10,9... | collective-permute-start | bytes 2359304 | tf_op jit(solution)/shard_map/ppermute | solution.py:81
  99.2 3.3 %fusion.34 = f32[1024,512]{1,0:T(8,128)} fusion(bf16[1024,384]{1,0:T(8,128)(2,1)} %bitcast.4, bf16[4096,512]{1,0:T(8,128)(2,1)} %pad_maximum_fusion, s32[]{:T(128)S(6)} %select_n.65), kind=kOutput, calls=%fused_computation.59 | convolution fusion | flops 402653184 | bytes 3276804 | tf_op jit(solution)/shard_map/dot_general | solution.py:16
  102.6 3.3 %fusion.32 = f32[1024,512]{1,0:T(8,128)} fusion(bf16[1024,384]{1,0:T(8,128)(2,1)} %collective-permute-done, bf16[4096,512]{1,0:T(8,128)(2,1)} %pad_maximum_fusion, s32[]{:T(128)S(6)} %select_n.68), kind=kOutput, calls=%fused_computation.57 | convolution fusion | flops 402653184 | bytes 3276804 | tf_op jit(solution)/shard_map/dot_general | solution.py:16
  105.8 3.2 %fusion.26 = f32[1024,512]{1,0:T(8,128)} fusion(bf16[1024,384]{1,0:T(8,128)(2,1)} %collective-permute-done.3, bf16[4096,512]{1,0:T(8,128)(2,1)} %pad_maximum_fusion, s32[]{:T(128)S(6)} %select_n.71), kind=kOutput, calls=%fused_computation.51 | convolution fusion | flops 402653184 | bytes 3276804 | tf_op jit(solution)/shard_map/dot_general | solution.py:16
  109.1 6.4 %collective-permute-done.5 = bf16[1024,384]{1,0:T(8,128)(2,1)S(1)} collective-permute-done((bf16[1024,384]{1,0:T(8,128)(2,1)}, bf16[1024,384]{1,0:T(8,128)(2,1)S(1)}, u32[]{:S(2)}, u32[]{:S(2)}) %collective-permute-start.5) | collective-permute-done | bytes 786464 | tf_op jit(solution)/shard_map/ppermute | solution.py:81
  115.5 3.4 %collective-permute-start.7 = (bf16[512,384]{1,0:T(8,128)(2,1)S(1)}, bf16[512,384]{1,0:T(8,128)(2,1)S(1)}, u32[]{:S(2)}, u32[]{:S(2)}) collective-permute-start(bf16[512,384]{1,0:T(8,128)(2,1)S(1)} %slice.62), channel_id=1, source_target_pairs={{0,7},{1,0},{2,1},{3,2},{4,3},{5,4},{6,5},{7,6},{8,15},{9,8},{10,9... | collective-permute-start | bytes 1179656 | tf_op jit(solution)/shard_map/ppermute | solution.py:88
  119.0 0.3 collective-permute-start.6
  119.3 3.2 %fusion.28 = f32[1024,512]{1,0:T(8,128)} fusion(bf16[1024,384]{1,0:T(8,128)(2,1)} %collective-permute-done.2, bf16[4096,512]{1,0:T(8,128)(2,1)} %pad_maximum_fusion, s32[]{:T(128)S(6)} %select_n.70), kind=kOutput, calls=%fused_computation.53 | convolution fusion | flops 402653184 | bytes 3276804 | tf_op jit(solution)/shard_map/dot_general | solution.py:16
  122.6 3.0 %fusion.24 = f32[1024,512]{1,0:T(8,128)} fusion(bf16[1024,384]{1,0:T(8,128)(2,1)S(1)} %collective-permute-done.4, bf16[4096,512]{1,0:T(8,128)(2,1)} %pad_maximum_fusion, s32[]{:T(128)S(6)} %select_n.72), kind=kOutput, calls=%fused_computation.49 | convolution fusion | flops 402653184 | bytes 3276804 | tf_op jit(solution)/shard_map/dot_general | solution.py:16
  125.6 3.5 %collective-permute-done.6 = bf16[512,384]{1,0:T(8,128)(2,1)S(1)} collective-permute-done((bf16[512,384]{1,0:T(8,128)(2,1)S(1)}, bf16[512,384]{1,0:T(8,128)(2,1)S(1)}, u32[]{:S(2)}, u32[]{:S(2)}) %collective-permute-start.6) | collective-permute-done | bytes 393248 | tf_op jit(solution)/shard_map/ppermute | solution.py:87
  129.1 3.0 %fusion.10 = f32[1024,512]{1,0:T(8,128)} fusion(bf16[512,384]{1,0:T(8,128)(2,1)S(1)} %collective-permute-done.7, bf16[512,384]{1,0:T(8,128)(2,1)S(1)} %collective-permute-done.6, bf16[4096,512]{1,0:T(8,128)(2,1)} %pad_maximum_fusion, s32[]{:T(128)S(6)} %select_n.74), kind=kOutput, calls=%fused_computation.32 | convolution fusion | flops 404226048 | bytes 3276804 | tf_op jit(solution)/shard_map/dot_general | solution.py:16
  132.1 3.2 %fusion.5 = f32[1024,512]{1,0:T(8,128)S(1)} fusion(bf16[1024,1024]{1,0:T(8,128)(2,1)} %bitcast.11, bf16[4096,512]{1,0:T(8,128)(2,1)} %pad_maximum_fusion), kind=kOutput, calls=%fused_computation.26 | convolution fusion | flops 1073741824 | bytes 5242880 | tf_op jit(solution)/shard_map/dot_general | solution.py:16
  135.4 0.5 copy-done.2
  135.9 0.6 copy-done.3
  136.6 3.8 %add_add_fusion = f32[1024,512]{1,0:T(8,128)S(1)} fusion(f32[1024,512]{1,0:T(8,128)} %fusion.10, f32[1024,512]{1,0:T(8,128)S(1)} %fusion.5, f32[1024,512]{1,0:T(8,128)} %fusion.24, f32[1024,512]{1,0:T(8,128)S(1)} %copy-done.2, f32[1024,512]{1,0:T(8,128)S(1)} %copy-done.3, f32[1024,512]{1,0:T(8,128)S(1)} %fusion.30, f32[1024,512]{1,0:T(8,128)S(1)} %copy-done, ...), kind=kOutput, calls=%fused_computation.1 | convolution fusion | flops 406847488 | bytes 20054020 | tf_op jit(solution)/shard_map/dot_general | solution.py:16
  140.5 0.3 fusion.4
  140.8 2.0 convolution_convert_fusion
  142.8 6.5 %all-to-all-start.2 = ((bf16[16,64,1024]{2,1,0:T(8,128)(2,1)}), bf16[16,64,1024]{2,1,0:T(8,128)(2,1)S(1)}, u32[]{:S(2)}, u32[]{:S(2)}) async-start(bf16[16,64,1024]{2,1,0:T(8,128)(2,1)} %bitcast.91), calls=%async_computation.2 | async-start | bytes 4194304 | tf_op jit(solution)/shard_map/all_to_all | solution.py:102
  149.3 1.4 convolution_convert_fusion.2
  150.7 1.0 fusion.82
  151.7 2.7 collective-permute-start.9
  154.3 8.8 %collective-permute-done.8 = bf16[512,384]{1,0:T(8,128)(2,1)S(1)} collective-permute-done((bf16[512,384]{1,0:T(8,128)(2,1)}, bf16[512,384]{1,0:T(8,128)(2,1)S(1)}, u32[]{:S(2)}, u32[]{:S(2)}) %collective-permute-start.8) | collective-permute-done | bytes 393248 | tf_op jit(solution)/shard_map/ppermute | solution.py:99
  163.1 2.4 add_convert_fusion.4
  165.5 2.5 collective-permute-start.12
  168.0 2.3 add_convert_fusion.6
  170.3 13.1 %collective-permute-done.12 = bf16[1024,384]{1,0:T(8,128)(2,1)} collective-permute-done((bf16[1024,384]{1,0:T(8,128)(2,1)}, bf16[1024,384]{1,0:T(8,128)(2,1)}, u32[]{:S(2)}, u32[]{:S(2)}) %collective-permute-start.12) | collective-permute-done | bytes 786464 | tf_op jit(solution)/shard_map/ppermute | solution.py:120
  183.5 2.6 add_convert_fusion.3
  186.0 3.4 %collective-permute-start.13 = (bf16[1024,384]{1,0:T(8,128)(2,1)}, bf16[1024,384]{1,0:T(8,128)(2,1)}, u32[]{:S(2)}, u32[]{:S(2)}) collective-permute-start(bf16[1024,384]{1,0:T(8,128)(2,1)} %add_convert_fusion.3), channel_id=1, source_target_pairs={{0,7},{1,0},{2,1},{3,2},{4,3},{5,4},{6,5},{7,6},{8,15},{9,8},{10,9... | collective-permute-start | bytes 2359304 | tf_op jit(solution)/shard_map/ppermute | solution.py:120
  189.4 2.6 add_convert_fusion.5
  192.0 12.0 %collective-permute-done.13 = bf16[1024,384]{1,0:T(8,128)(2,1)} collective-permute-done((bf16[1024,384]{1,0:T(8,128)(2,1)}, bf16[1024,384]{1,0:T(8,128)(2,1)}, u32[]{:S(2)}, u32[]{:S(2)}) %collective-permute-start.13) | collective-permute-done | bytes 786464 | tf_op jit(solution)/shard_map/ppermute | solution.py:120
  204.0 2.6 add_convert_fusion.1
  206.6 3.4 %collective-permute-start.15 = (bf16[1024,384]{1,0:T(8,128)(2,1)}, bf16[1024,384]{1,0:T(8,128)(2,1)}, u32[]{:S(2)}, u32[]{:S(2)}) collective-permute-start(bf16[1024,384]{1,0:T(8,128)(2,1)} %add_convert_fusion.1), channel_id=1, source_target_pairs={{0,7},{1,0},{2,1},{3,2},{4,3},{5,4},{6,5},{7,6},{8,15},{9,8},{10,9... | collective-permute-start | bytes 2359304 | tf_op jit(solution)/shard_map/ppermute | solution.py:120
  210.0 2.6 add_convert_fusion.2
  212.6 0.7 fusion.86
  213.3 0.3 copy-done.5
  213.6 0.7 fusion.1
  214.4 0.9 copy.22
  215.3 4.0 %all-to-all-start.3 = ((bf16[8,256,128]{2,1,0:T(8,128)(2,1)}), bf16[8,256,128]{2,1,0:T(8,128)(2,1)S(1)}, u32[]{:S(2)}, u32[]{:S(2)}) async-start(bf16[8,256,128]{2,1,0:T(8,128)(2,1)} %bitcast.88), calls=%async_computation.3 | async-start | bytes 1048576 | tf_op jit(solution)/shard_map/all_to_all | solution.py:128
  219.2 1.4 fusion.38
  220.6 3.3 %collective-permute-done.15 = bf16[1024,384]{1,0:T(8,128)(2,1)} collective-permute-done((bf16[1024,384]{1,0:T(8,128)(2,1)}, bf16[1024,384]{1,0:T(8,128)(2,1)}, u32[]{:S(2)}, u32[]{:S(2)}) %collective-permute-start.15) | collective-permute-done | bytes 786464 | tf_op jit(solution)/shard_map/ppermute | solution.py:120
  223.9 6.7 %collective-permute-done.14 = bf16[1024,384]{1,0:T(8,128)(2,1)} collective-permute-done((bf16[1024,384]{1,0:T(8,128)(2,1)}, bf16[1024,384]{1,0:T(8,128)(2,1)}, u32[]{:S(2)}, u32[]{:S(2)}) %collective-permute-start.14) | collective-permute-done | bytes 786464 | tf_op jit(solution)/shard_map/ppermute | solution.py:119
  230.6 2.6 add_convert_fusion
  233.2 4.0 %all-to-all-done.3 = bf16[8,256,128]{2,1,0:T(8,128)(2,1)S(1)} async-done(((bf16[8,256,128]{2,1,0:T(8,128)(2,1)}), bf16[8,256,128]{2,1,0:T(8,128)(2,1)S(1)}, u32[]{:S(2)}, u32[]{:S(2)}) %all-to-all-start.3) | async-done | bytes 524320 | tf_op jit(solution)/shard_map/all_to_all | solution.py:128
  237.2 16.0 %all-to-all-start.4 = ((bf16[16,64,384]{2,1,0:T(8,128)(2,1)}), bf16[16,64,384]{2,1,0:T(8,128)(2,1)S(1)}, u32[]{:S(2)}, u32[]{:S(2)}) async-start(bf16[16,64,384]{2,1,0:T(8,128)(2,1)} %bitcast.23), calls=%async_computation.4 | async-start | bytes 1572864 | tf_op jit(solution)/shard_map/all_to_all | solution.py:130
  253.3 22.6 %all-to-all-done.4 = bf16[16,64,384]{2,1,0:T(8,128)(2,1)S(1)} async-done(((bf16[16,64,384]{2,1,0:T(8,128)(2,1)}), bf16[16,64,384]{2,1,0:T(8,128)(2,1)S(1)}, u32[]{:S(2)}, u32[]{:S(2)}) %all-to-all-start.4) | async-done | bytes 786464 | tf_op jit(solution)/shard_map/all_to_all | solution.py:130
  275.9 0.5 fusion.87
  276.4 0.5 fusion.85
  277.1 9.1 %all_to_all.30 = f32[8,2,256]{2,1,0:T(2,128)S(1)} all-to-all(f32[8,2,256]{2,1,0:T(2,128)S(1)} %broadcast_in_dim.49), channel_id=1, replica_groups=mesh['grp'=2,'ep'=16,'tp'=8] {'tp'}, dimensions={0} | all-to-all | bytes 32768 | tf_op jit(solution)/shard_map/all_to_all | solution.py:134
  286.3 0.9 add_convert_fusion.7
  (55 shorter events, 1.1 us)
Async XLA Ops:
  0.0 27.7 %copy-start.4 = (bf16[1,256,4096]{2,1,0:T(8,128)(2,1)S(1)}, bf16[1,256,4096]{2,1,0:T(8,128)(2,1)}, u32[]{:S(2)}) copy-start(bf16[1,256,4096]{2,1,0:T(8,128)(2,1)} %param.13) | copy-start | bytes 6291460
  3.3 47.3 %all-to-all-start = ((bf16[16,64,384]{2,1,0:T(8,128)(2,1)}), bf16[16,64,384]{2,1,0:T(8,128)(2,1)}, u32[]{:S(2)}, u32[]{:S(2)}) async-start(bf16[16,64,384]{2,1,0:T(8,128)(2,1)} %bitcast.3), calls=%async_computation | async-start | bytes 1572864 | tf_op jit(solution)/shard_map/all_to_all | solution.py:66
  28.6 0.7 copy-start.13
  28.7 4.9 %copy-start.8 = (bf16[1,4096,256]{2,1,0:T(8,128)(2,1)S(1)}, bf16[1,4096,256]{2,1,0:T(8,128)(2,1)}, u32[]{:S(2)}) copy-start(bf16[1,4096,256]{2,1,0:T(8,128)(2,1)} %param.11) | copy-start | bytes 6291460
  28.8 4.8 %copy-start.7 = (bf16[1,4096,256]{2,1,0:T(8,128)(2,1)S(1)}, bf16[1,4096,256]{2,1,0:T(8,128)(2,1)}, u32[]{:S(2)}) copy-start(bf16[1,4096,256]{2,1,0:T(8,128)(2,1)} %param.12) | copy-start | bytes 6291460
  50.6 81.5 %all-to-all-start.1 = ((bf16[16,64,1024]{2,1,0:T(8,128)(2,1)}), bf16[16,64,1024]{2,1,0:T(8,128)(2,1)}, u32[]{:S(2)}, u32[]{:S(2)}) async-start(bf16[16,64,1024]{2,1,0:T(8,128)(2,1)} %bitcast.5), calls=%async_computation.1 | async-start | bytes 4194304 | tf_op jit(solution)/shard_map/all_to_all | solution.py:72
  55.1 20.6 %collective-permute-start = (bf16[1024,384]{1,0:T(8,128)(2,1)}, bf16[1024,384]{1,0:T(8,128)(2,1)}, u32[]{:S(2)}, u32[]{:S(2)}) collective-permute-start(bf16[1024,384]{1,0:T(8,128)(2,1)} %bitcast.4), channel_id=1, source_target_pairs={{0,1},{1,2},{2,3},{3,4},{4,5},{5,6},{6,7},{7,0},{8,9},{9,10},{10,1... | collective-permute-start | bytes 2359304 | tf_op jit(solution)/shard_map/ppermute | solution.py:80
  55.3 20.5 %collective-permute-start.1 = (bf16[1024,384]{1,0:T(8,128)(2,1)}, bf16[1024,384]{1,0:T(8,128)(2,1)}, u32[]{:S(2)}, u32[]{:S(2)}) collective-permute-start(bf16[1024,384]{1,0:T(8,128)(2,1)} %bitcast.4), channel_id=1, source_target_pairs={{0,7},{1,0},{2,1},{3,2},{4,3},{5,4},{6,5},{7,6},{8,15},{9,8},{10,9... | collective-permute-start | bytes 2359304 | tf_op jit(solution)/shard_map/ppermute | solution.py:81
  75.8 20.0 %collective-permute-start.3 = (bf16[1024,384]{1,0:T(8,128)(2,1)}, bf16[1024,384]{1,0:T(8,128)(2,1)}, u32[]{:S(2)}, u32[]{:S(2)}) collective-permute-start(bf16[1024,384]{1,0:T(8,128)(2,1)} %collective-permute-done.1), channel_id=1, source_target_pairs={{0,7},{1,0},{2,1},{3,2},{4,3},{5,4},{6,5},{7,6},{8,15},{9,8},{10,9... | collective-permute-start | bytes 2359304 | tf_op jit(solution)/shard_map/ppermute | solution.py:81
  78.7 20.5 %collective-permute-start.2 = (bf16[1024,384]{1,0:T(8,128)(2,1)}, bf16[1024,384]{1,0:T(8,128)(2,1)}, u32[]{:S(2)}, u32[]{:S(2)}) collective-permute-start(bf16[1024,384]{1,0:T(8,128)(2,1)} %collective-permute-done), channel_id=1, source_target_pairs={{0,1},{1,2},{2,3},{3,4},{4,5},{5,6},{6,7},{7,0},{8,9},{9,10},{10,1... | collective-permute-start | bytes 2359304 | tf_op jit(solution)/shard_map/ppermute | solution.py:80
  95.8 19.7 %collective-permute-start.5 = (bf16[1024,384]{1,0:T(8,128)(2,1)}, bf16[1024,384]{1,0:T(8,128)(2,1)S(1)}, u32[]{:S(2)}, u32[]{:S(2)}) collective-permute-start(bf16[1024,384]{1,0:T(8,128)(2,1)} %collective-permute-done.3), channel_id=1, source_target_pairs={{0,7},{1,0},{2,1},{3,2},{4,3},{5,4},{6,5},{7,6},{8,15},{9,8},{10,9... | collective-permute-start | bytes 2359304 | tf_op jit(solution)/shard_map/ppermute | solution.py:81
  99.2 19.7 %collective-permute-start.4 = (bf16[1024,384]{1,0:T(8,128)(2,1)}, bf16[1024,384]{1,0:T(8,128)(2,1)S(1)}, u32[]{:S(2)}, u32[]{:S(2)}) collective-permute-start(bf16[1024,384]{1,0:T(8,128)(2,1)} %collective-permute-done.2), channel_id=1, source_target_pairs={{0,1},{1,2},{2,3},{3,4},{4,5},{5,6},{6,7},{7,0},{8,9},{9,10},{10,1... | collective-permute-start | bytes 2359304 | tf_op jit(solution)/shard_map/ppermute | solution.py:80
  115.5 7.1 %copy-start.9 = (bf16[1024,384]{1,0:T(8,128)(2,1)}, bf16[1024,384]{1,0:T(8,128)(2,1)S(1)}, u32[]{:S(2)}) copy-start(bf16[1024,384]{1,0:T(8,128)(2,1)S(1)} %collective-permute-done.5) | copy-start | bytes 2359300
  115.5 10.1 %collective-permute-start.7 = (bf16[512,384]{1,0:T(8,128)(2,1)S(1)}, bf16[512,384]{1,0:T(8,128)(2,1)S(1)}, u32[]{:S(2)}, u32[]{:S(2)}) collective-permute-start(bf16[512,384]{1,0:T(8,128)(2,1)S(1)} %slice.62), channel_id=1, source_target_pairs={{0,7},{1,0},{2,1},{3,2},{4,3},{5,4},{6,5},{7,6},{8,15},{9,8},{10,9... | collective-permute-start | bytes 1179656 | tf_op jit(solution)/shard_map/ppermute | solution.py:88
  119.0 10.1 %collective-permute-start.6 = (bf16[512,384]{1,0:T(8,128)(2,1)S(1)}, bf16[512,384]{1,0:T(8,128)(2,1)S(1)}, u32[]{:S(2)}, u32[]{:S(2)}) collective-permute-start(bf16[512,384]{1,0:T(8,128)(2,1)S(1)} %slice.61), channel_id=1, source_target_pairs={{0,1},{1,2},{2,3},{3,4},{4,5},{5,6},{6,7},{7,0},{8,9},{9,10},{10,1... | collective-permute-start | bytes 1179656 | tf_op jit(solution)/shard_map/ppermute | solution.py:87
  132.1 3.3 %copy-start = (f32[1024,512]{1,0:T(8,128)S(1)}, f32[1024,512]{1,0:T(8,128)}, u32[]{:S(2)}) copy-start(f32[1024,512]{1,0:T(8,128)} %fusion.34) | copy-start | bytes 6291460
  132.1 3.3 %copy-start.1 = (f32[1024,512]{1,0:T(8,128)S(1)}, f32[1024,512]{1,0:T(8,128)}, u32[]{:S(2)}) copy-start(f32[1024,512]{1,0:T(8,128)} %fusion.32) | copy-start | bytes 6291460
  132.1 3.8 %copy-start.2 = (f32[1024,512]{1,0:T(8,128)S(1)}, f32[1024,512]{1,0:T(8,128)}, u32[]{:S(2)}) copy-start(f32[1024,512]{1,0:T(8,128)} %fusion.26) | copy-start | bytes 6291460
  132.1 4.4 %copy-start.3 = (f32[1024,512]{1,0:T(8,128)S(1)}, f32[1024,512]{1,0:T(8,128)}, u32[]{:S(2)}) copy-start(f32[1024,512]{1,0:T(8,128)} %fusion.28) | copy-start | bytes 6291460
  132.1 4.5 %copy-start.10 = (bf16[1024,384]{1,0:T(8,128)(2,1)S(1)}, bf16[1024,384]{1,0:T(8,128)(2,1)}, u32[]{:S(2)}) copy-start(bf16[1024,384]{1,0:T(8,128)(2,1)} %copy-done.9) | copy-start | bytes 2359300
  142.8 69.7 %all-to-all-start.2 = ((bf16[16,64,1024]{2,1,0:T(8,128)(2,1)}), bf16[16,64,1024]{2,1,0:T(8,128)(2,1)S(1)}, u32[]{:S(2)}, u32[]{:S(2)}) async-start(bf16[16,64,1024]{2,1,0:T(8,128)(2,1)} %bitcast.91), calls=%async_computation.2 | async-start | bytes 4194304 | tf_op jit(solution)/shard_map/all_to_all | solution.py:102
  151.7 11.4 %collective-permute-start.8 = (bf16[512,384]{1,0:T(8,128)(2,1)}, bf16[512,384]{1,0:T(8,128)(2,1)S(1)}, u32[]{:S(2)}, u32[]{:S(2)}) collective-permute-start(bf16[512,384]{1,0:T(8,128)(2,1)} %get-tuple-element.44), channel_id=1, source_target_pairs={{0,1},{1,2},{2,3},{3,4},{4,5},{5,6},{6,7},{7,0},{8,9},{9,10},{10,1... | collective-permute-start | bytes 1179656 | tf_op jit(solution)/shard_map/ppermute | solution.py:99
  151.7 11.4 %collective-permute-start.9 = (bf16[512,384]{1,0:T(8,128)(2,1)}, bf16[512,384]{1,0:T(8,128)(2,1)}, u32[]{:S(2)}, u32[]{:S(2)}) collective-permute-start(bf16[512,384]{1,0:T(8,128)(2,1)} %get-tuple-element.43), channel_id=1, source_target_pairs={{0,7},{1,0},{2,1},{3,2},{4,3},{5,4},{6,5},{7,6},{8,15},{9,8},{10,9... | collective-permute-start | bytes 1179656 | tf_op jit(solution)/shard_map/ppermute | solution.py:100
  165.5 17.9 %collective-permute-start.12 = (bf16[1024,384]{1,0:T(8,128)(2,1)}, bf16[1024,384]{1,0:T(8,128)(2,1)}, u32[]{:S(2)}, u32[]{:S(2)}) collective-permute-start(bf16[1024,384]{1,0:T(8,128)(2,1)} %add_convert_fusion.4), channel_id=1, source_target_pairs={{0,7},{1,0},{2,1},{3,2},{4,3},{5,4},{6,5},{7,6},{8,15},{9,8},{10,9... | collective-permute-start | bytes 2359304 | tf_op jit(solution)/shard_map/ppermute | solution.py:120
  170.3 19.1 %collective-permute-start.10 = (bf16[1024,384]{1,0:T(8,128)(2,1)}, bf16[1024,384]{1,0:T(8,128)(2,1)}, u32[]{:S(2)}, u32[]{:S(2)}) collective-permute-start(bf16[1024,384]{1,0:T(8,128)(2,1)} %add_convert_fusion.6), channel_id=1, source_target_pairs={{0,1},{1,2},{2,3},{3,4},{4,5},{5,6},{6,7},{7,0},{8,9},{9,10},{10,1... | collective-permute-start | bytes 2359304 | tf_op jit(solution)/shard_map/ppermute | solution.py:119
  186.0 18.0 %collective-permute-start.13 = (bf16[1024,384]{1,0:T(8,128)(2,1)}, bf16[1024,384]{1,0:T(8,128)(2,1)}, u32[]{:S(2)}, u32[]{:S(2)}) collective-permute-start(bf16[1024,384]{1,0:T(8,128)(2,1)} %add_convert_fusion.3), channel_id=1, source_target_pairs={{0,7},{1,0},{2,1},{3,2},{4,3},{5,4},{6,5},{7,6},{8,15},{9,8},{10,9... | collective-permute-start | bytes 2359304 | tf_op jit(solution)/shard_map/ppermute | solution.py:120
  192.0 18.0 %collective-permute-start.11 = (bf16[1024,384]{1,0:T(8,128)(2,1)}, bf16[1024,384]{1,0:T(8,128)(2,1)}, u32[]{:S(2)}, u32[]{:S(2)}) collective-permute-start(bf16[1024,384]{1,0:T(8,128)(2,1)} %add_convert_fusion.5), channel_id=1, source_target_pairs={{0,1},{1,2},{2,3},{3,4},{4,5},{5,6},{6,7},{7,0},{8,9},{9,10},{10,1... | collective-permute-start | bytes 2359304 | tf_op jit(solution)/shard_map/ppermute | solution.py:119
  206.6 17.3 %collective-permute-start.15 = (bf16[1024,384]{1,0:T(8,128)(2,1)}, bf16[1024,384]{1,0:T(8,128)(2,1)}, u32[]{:S(2)}, u32[]{:S(2)}) collective-permute-start(bf16[1024,384]{1,0:T(8,128)(2,1)} %add_convert_fusion.1), channel_id=1, source_target_pairs={{0,7},{1,0},{2,1},{3,2},{4,3},{5,4},{6,5},{7,6},{8,15},{9,8},{10,9... | collective-permute-start | bytes 2359304 | tf_op jit(solution)/shard_map/ppermute | solution.py:120
  212.6 18.0 %collective-permute-start.14 = (bf16[1024,384]{1,0:T(8,128)(2,1)}, bf16[1024,384]{1,0:T(8,128)(2,1)}, u32[]{:S(2)}, u32[]{:S(2)}) collective-permute-start(bf16[1024,384]{1,0:T(8,128)(2,1)} %add_convert_fusion.2), channel_id=1, source_target_pairs={{0,1},{1,2},{2,3},{3,4},{4,5},{5,6},{6,7},{7,0},{8,9},{9,10},{10,1... | collective-permute-start | bytes 2359304 | tf_op jit(solution)/shard_map/ppermute | solution.py:119
  212.6 1.0 copy-start.5
  215.3 21.9 %all-to-all-start.3 = ((bf16[8,256,128]{2,1,0:T(8,128)(2,1)}), bf16[8,256,128]{2,1,0:T(8,128)(2,1)S(1)}, u32[]{:S(2)}, u32[]{:S(2)}) async-start(bf16[8,256,128]{2,1,0:T(8,128)(2,1)} %bitcast.88), calls=%async_computation.3 | async-start | bytes 1048576 | tf_op jit(solution)/shard_map/all_to_all | solution.py:128
  233.2 43.2 %copy-start.6 = (bf16[1024,256]{1,0:T(8,128)(2,1)S(1)}, bf16[1024,256]{1,0:T(8,128)(2,1)}, u32[]{:S(2)}) copy-start(bf16[1024,256]{1,0:T(8,128)(2,1)} %get-tuple-element.36) | copy-start | bytes 1572868
  237.2 38.7 %all-to-all-start.4 = ((bf16[16,64,384]{2,1,0:T(8,128)(2,1)}), bf16[16,64,384]{2,1,0:T(8,128)(2,1)S(1)}, u32[]{:S(2)}, u32[]{:S(2)}) async-start(bf16[16,64,384]{2,1,0:T(8,128)(2,1)} %bitcast.23), calls=%async_computation.4 | async-start | bytes 1572864 | tf_op jit(solution)/shard_map/all_to_all | solution.py:130
  275.9 10.3 %copy-start.11 = (f32[512]{0:T(512)S(1)}, f32[512]{0:T(512)}, u32[]{:S(2)}) copy-start(f32[512]{0:T(512)} %param.15) | copy-start | bytes 6148
  275.9 10.4 %copy-start.12 = (f32[512]{0:T(512)S(1)}, f32[512]{0:T(512)}, u32[]{:S(2)}) copy-start(f32[512]{0:T(512)} %param.14) | copy-start | bytes 6148
where the time goes:
time: 288 us; the launch traced here: 287 us
  waiting for transfers between devices  128 us (44%)
  starting transfers between devices  80.3 us (28%)
  matrix products  55.9 us (19%)
  blocking collectives  9.11 us (3%)
  other arithmetic  7.54 us (3%)
  local copies, waits for them, and re-layouts  5.95 us (2%)
    dot_general x25, matrix products, f32_dot(): return lax.dot_general(a, b, dims, preferred_element_type=jnp.float32)  55.9 us
    ppermute x3, waiting for transfers between devices, layer(): seen_left.append(lax.ppermute(to_left, 'tp', left))  28.5 us
    all_to_all x1, starting transfers between devices, layer(): lax.all_to_all(out1, 'ep', 0, 0, tiled=True).reshape(rows, ring_piece)  24.4 us
    all_to_all x1, waiting for transfers between devices, layer(): lax.all_to_all(back1.reshape(n_ep, CAP, ring_piece), 'ep', 0, 0, tiled=True)  22.6 us
    ppermute x3, waiting for transfers between devices, layer(): to_left = lax.ppermute(to_left, 'tp', left)  21.6 us
    ppermute x3, waiting for transfers between devices, layer(): to_right = lax.ppermute(to_right, 'tp', right)  17.9 us
    all_to_all x1, starting transfers between devices, layer(): lax.all_to_all(back1.reshape(n_ep, CAP, ring_piece), 'ep', 0, 0, tiled=True)  16 us
    all_to_all x1, waiting for transfers between devices, layer(): lax.all_to_all(out1, 'ep', 0, 0, tiled=True).reshape(rows, ring_piece)  14.7 us
  transfers between devices with their start and end apart: 21, of which 12 were waited for; matrix products, arithmetic and copies ran while one was open for 18% of the time, Pallas kernels for 0%

commit v1 on v0

v1 whole, which is shorter than its diff:
```python
import jax
import jax.numpy as jnp
from jax import lax
from jax.experimental import pallas as pl
from jax.sharding import PartitionSpec as P

D = 4096
EXPERTS = 16
CAP = 64
RING_PARTS = 3
ALL_PARTS = 4
GROUPS = 2

norm_eps = 1e-05


def f32_dot(a, b, dims=(((1,), (0,)), ((), ()))):
    return lax.dot_general(a, b, dims, preferred_element_type=jnp.float32)


def route(expert_ids, gates):
    ids = expert_ids.T
    tok = ids.shape[1]
    experts = jnp.arange(EXPERTS, dtype=jnp.int32)[:, None]
    first = ids[0][None, :] == experts
    second = ids[1][None, :] == experts
    named = jnp.logical_or(first, second).astype(jnp.bfloat16)
    row = jnp.arange(tok, dtype=jnp.int32)
    before = (row[:, None] < row[None, :]).astype(jnp.bfloat16)
    slot = f32_dot(named, before).astype(jnp.int32) + experts * CAP
    target0 = jnp.sum(jnp.where(first, slot, 0), axis=0)
    target1 = jnp.sum(jnp.where(second, slot, 0), axis=0)
    slots = jnp.arange(EXPERTS * CAP, dtype=jnp.int32)[:, None]
    at0 = slots == target0[None, :]
    at1 = slots == target1[None, :]
    send = jnp.logical_or(at0, at1).astype(jnp.bfloat16)
    g = gates.T
    weight = jnp.where(at0, g[0][None, :], 0.0) + jnp.where(at1, g[1][None, :], 0.0)
    high = lax.reduce_precision(weight, 8, 7)
    return send, high.astype(jnp.bfloat16), (weight - high).astype(jnp.bfloat16)


def down_kernel(hidden, weights, ring_out, flat_out):
    ring_piece = ring_out.shape[2]
    part = f32_dot(hidden[...], weights[...]).astype(jnp.bfloat16)
    ring_out[0] = part[:, :ring_piece]
    flat_out[...] = part[:, ring_piece:]


def down(hidden, weights, pieces, ring_piece):
    rows, inner = hidden.shape
    piece = weights.shape[1] // pieces
    flat_piece = piece - ring_piece
    return pl.pallas_call(
        down_kernel,
        grid=(pieces,),
        in_specs=[
            pl.BlockSpec((rows, inner), lambda i: (0, 0)),
            pl.BlockSpec((inner, piece), lambda i: (0, i)),
        ],
        out_specs=[
            pl.BlockSpec((1, rows, ring_piece), lambda i: (i, 0, 0)),
            pl.BlockSpec((rows, flat_piece), lambda i: (0, i)),
        ],
        out_shape=[
            jax.ShapeDtypeStruct((pieces, rows, ring_piece), jnp.bfloat16),
            jax.ShapeDtypeStruct((rows, flat_piece * pieces), jnp.bfloat16),
        ],
        cost_estimate=pl.CostEstimate(
            flops=2 * rows * inner * piece * pieces,
            transcendentals=0,
            bytes_accessed=2 * (rows * inner + inner * piece * pieces + rows * piece * pieces),
        ),
        name="down",
    )(hidden, weights)


def layer(tokens, expert_ids, gates, w_gate, w_up, w_down, norm_gain, norm_bias):
    n_tp = lax.axis_size("tp")
    n_ep = lax.axis_size("ep")
    me = lax.axis_index("tp")
    piece = norm_gain.shape[0]
    ring_piece = piece * RING_PARTS // ALL_PARTS
    flat_piece = piece - ring_piece
    ring_width = ring_piece * n_tp
    flat_width = flat_piece * n_tp
    wd = w_down[0]
    part_rows = CAP // GROUPS
    group = n_ep * part_rows
    hidden_width = w_up.shape[2]
    send, weight_high, weight_low = route(expert_ids, gates)
    own = lax.dynamic_slice_in_dim(tokens, me * ring_piece, ring_piece, 1)

    def group_of(x, h):
        return x.reshape(n_ep, CAP, x.shape[-1])[:, h * part_rows : (h + 1) * part_rows].reshape(group, x.shape[-1])

    arrived = []
    for h in range(GROUPS):
        out = f32_dot(group_of(send, h), own).astype(jnp.bfloat16).reshape(n_ep, part_rows, ring_piece)
        arrived.append(lax.all_to_all(out, "ep", 0, 0, tiled=True).reshape(group, ring_piece))
    out = f32_dot(send, tokens[:, ring_width:]).astype(jnp.bfloat16).reshape(n_ep, CAP, flat_width)
    w_both = jnp.concatenate([w_gate[0], w_up[0]], axis=1)
    arrived[-1], out, w_both, weight_high, weight_low = lax.optimization_barrier(
        (arrived[-1], out, w_both, weight_high, weight_low)
    )
    flat = lax.all_to_all(out, "ep", 0, 0, tiled=True)

    whole = []
    for h in range(GROUPS):
        whole.append(lax.all_gather(arrived[h], "tp", axis=1, tiled=True))
    hidden = []
    for h in range(GROUPS):
        acc = f32_dot(whole[h], w_both[:ring_width]) + f32_dot(group_of(flat, h), w_both[ring_width:])
        g = acc[:, :hidden_width]
        u = acc[:, hidden_width:]
        hidden.append((g / (1.0 + jnp.exp(-g)) * u).astype(jnp.bfloat16))

    back = []
    back2 = []
    for x in hidden:
        ring_part, flat_part = down(x, wd, n_tp, ring_piece)
        back.append(ring_part)
        back2.append(flat_part.reshape(n_ep, part_rows, flat_width))
    for h in range(GROUPS - 1):
        back[h], whole[-1] = lax.optimization_barrier((back[h], whole[-1]))
    summed = []
    for h in range(GROUPS):
        summed.append(lax.psum_scatter(back[h], "tp", scatter_dimension=0))
    back2 = jnp.concatenate(back2, axis=1)
    flat = lax.all_to_all(back2, "ep", 0, 0, tiled=True).reshape(n_ep * CAP, flat_width)

    first_dims = (((0,), (0,)), ((), ()))
    mixed2 = f32_dot(weight_high, flat, first_dims) + f32_dot(weight_low, flat, first_dims)
    mixed2 = lax.psum_scatter(mixed2.astype(jnp.bfloat16), "tp", scatter_dimension=1, tiled=True)
    mixed1 = 0.0
    for h in range(GROUPS):
        home = lax.all_to_all(summed[h].reshape(n_ep, part_rows, ring_piece), "ep", 0, 0, tiled=True)
        home = home.reshape(group, ring_piece)
        for weight in (weight_high, weight_low):
            mixed1 = mixed1 + f32_dot(group_of(weight, h), home, first_dims)
    combined = jnp.concatenate([mixed1, mixed2.astype(jnp.float32)], axis=1)

    stats = jnp.stack([jnp.sum(combined, axis=1), jnp.sum(combined * combined, axis=1)])
    stats = lax.all_to_all(jnp.broadcast_to(stats[None], (n_tp, *stats.shape)), "tp", 0, 0, tiled=True)
    stats = jnp.sum(stats, axis=0)
    row_mean = stats[0] / D
    row_var = stats[1] / D - row_mean * row_mean
    normed = (combined - row_mean[:, None]) * lax.rsqrt(
        row_var[:, None] + norm_eps
    ) * norm_gain + norm_bias
    return normed.astype(jnp.bfloat16)


def solution(mesh):
    return jax.shard_map(
        layer,
        mesh=mesh,
        in_specs=(
            P(("grp", "ep"), None),
            P(("grp", "ep"), None),
            P(("grp", "ep"), None),
            P("ep", None, "tp"),
            P("ep", None, "tp"),
            P("ep", "tp", None),
            P("tp"),
            P("tp"),
        ),
        out_specs=P(("grp", "ep"), "tp"),
        check_vma=False,
    )
```

time: 288 us -> 304 us (1.056); the launches traced: 287 us -> 299 us
  blocking collectives: 9.11 us -> 143 us
  waiting for transfers between devices: 128 us -> 55.1 us
  starting transfers between devices: 80.3 us -> 39 us
  matrix products: 55.9 us -> 21.4 us
  Pallas kernels: 0 us -> 14.4 us
  between operations: 0.27 us -> 13.4 us
    all_to_all x0 -> x3, blocking collectives: none -> 131 us  [the longest x1 60.6 us: layer(): lax.all_to_all(back2, 'ep', 0, 0, tiled=True)]
    ppermute x16 -> x0, waiting for transfers between devices: 86.8 us -> none  [the longest x3 28.5 us: layer(): seen_left.append(lax.ppermute(to_left, 'tp', left))]
    dot_general x25 -> x14, matrix products: 55.9 us -> 21.4 us  [f32_dot(): return lax.dot_general(a, b, dims, preferred_element_type=jnp.float32)]
    all_to_all x5 -> x3, waiting for transfers between devices: 41.2 us -> 8.45 us  [the longest x1 8.45 us: layer(): lax.all_to_all(out, 'ep', 0, 0, tiled=True).reshape(group, ring_piece)]
    unnamed x0 -> x6, waiting for transfers between devices: none -> 28.7 us
    ppermute x16 -> x0, starting transfers between devices: 24.9 us -> none  [the longest x3 9.32 us: layer(): seen_left.append(lax.ppermute(to_left, 'tp', left))]
    all_to_all x5 -> x3, starting transfers between devices: 55.4 us -> 38.7 us  [the longest x1 23.8 us: layer(): lax.all_to_all(out, 'ep', 0, 0, tiled=True).reshape(group, ring_piece)]
    reduce_scatter x0 -> x2, waiting for transfers between devices: none -> 15.5 us  [layer(): summed.append(lax.psum_scatter(back[h], 'tp', scatter_dimension=0))]
  transfers between devices with their start and end apart: 21 -> 8, of which waited for: 12 -> 4; matrix products, arithmetic and copies ran while one was open for 18% -> 9% of each run, Pallas kernels for 0% -> 5%
where the time goes in v1:
time: 304 us; the launch traced here: 299 us
  blocking collectives  143 us (47%)
  waiting for transfers between devices  55.1 us (18%)
  starting transfers between devices  39 us (13%)
  matrix products  21.4 us (7%)
  Pallas kernels  14.4 us (5%)
  between operations  13.4 us (4%)
  other arithmetic  7.56 us (2%)
  local copies, waits for them, and re-layouts  5.63 us (2%)
    all_to_all x1, blocking collectives, layer(): lax.all_to_all(back2, 'ep', 0, 0, tiled=True)  60.6 us
    all_to_all x1, blocking collectives, layer(): flat = lax.all_to_all(out, 'ep', 0, 0, tiled=True)  53.7 us
    unnamed x6, waiting for transfers between devices  28.7 us
    all_to_all x1, starting transfers between devices, layer(): lax.all_to_all(out, 'ep', 0, 0, tiled=True).reshape(group, ring_piece)  23.8 us
    dot_general x14, matrix products, f32_dot(): return lax.dot_general(a, b, dims, preferred_element_type=jnp.float32)  21.4 us
    all_to_all x1, blocking collectives, layer(): lax.all_to_all(out, 'ep', 0, 0, tiled=True).reshape(group, ring_piece)  17.2 us
    reduce_scatter x2, waiting for transfers between devices, layer(): summed.append(lax.psum_scatter(back[h], 'tp', scatter_dimension=0))  15.5 us
    all_to_all x2, starting transfers between devices, layer(): lax.all_to_all(summed[h].reshape(n_ep, part_rows, ring_piece), 'ep', 0, 0...  14.9 us
  transfers between devices with their start and end apart: 8, of which 4 were waited for; matrix products, arithmetic and copies ran while one was open for 9% of the time, Pallas kernels for 5%

profile of v1, /device:TPU:513, one launch (start us, length us, event | category | flops | bytes accessed | tf_op | source)
XLA Modules:
  0.0 299.1 jit_solution(5670896576779993717)
XLA Ops:
  6.6 0.8 fusion.34
  7.3 0.2 select_reduce_fusion.1
  7.5 0.2 compare_or_fusion
  7.7 0.8 fusion.32
  8.6 2.0 convolution_convert_fusion.2
  10.6 23.8 %all-to-all-start = ((bf16[16,32,384]{2,1,0:T(8,128)(2,1)}), bf16[16,32,384]{2,1,0:T(8,128)(2,1)S(1)}, u32[]{:S(2)}, u32[]{:S(2)}) async-start(bf16[16,32,384]{2,1,0:T(8,128)(2,1)} %bitcast.4), calls=%async_computation | async-start | bytes 786432 | tf_op jit(solution)/shard_map/all_to_all | solution.py:100
  34.3 0.1 all-gather.5.cloned.1.call-start
  34.4 0.0 copy-start
  34.4 1.9 convolution_convert_fusion
  36.3 0.0 copy-done.6
  36.4 0.3 fusion.9
  36.7 0.0 copy-done
  36.7 3.9 %pad_maximum_fusion = bf16[4096,512]{1,0:T(8,128)(2,1)} fusion(bf16[4096,256]{1,0:T(8,128)(2,1)S(1)} %bitcast.67, bf16[4096,256]{1,0:T(8,128)(2,1)} %bitcast.68), kind=kLoop, calls=%fused_computation | loop fusion | flops 8388608 | bytes 8388608 | tf_op jit(solution)/shard_map/concatenate | solution.py:102
  40.6 8.4 %all-to-all-done = bf16[16,32,384]{2,1,0:T(8,128)(2,1)S(1)} async-done(((bf16[16,32,384]{2,1,0:T(8,128)(2,1)}), bf16[16,32,384]{2,1,0:T(8,128)(2,1)S(1)}, u32[]{:S(2)}, u32[]{:S(2)}) %all-to-all-start) | async-done | bytes 393248 | tf_op jit(solution)/shard_map/all_to_all | solution.py:100
  49.0 0.8 copy-done.1
  49.8 0.1 all-gather.5.cloned.1.call-update
  49.9 0.1 all-gather.3.cloned.1.call-start
  49.9 1.3 convolution_convert_fusion.1
  51.3 17.2 %all_to_all.35 = bf16[16,32,384]{2,1,0:T(8,128)(2,1)} all-to-all(bf16[16,32,384]{2,1,0:T(8,128)(2,1)S(1)} %bitcast.73), channel_id=1, replica_groups=mesh['grp'=2,'ep'=16,'tp'=8] {'ep'}, dimensions={0} | all-to-all | bytes 786432 | tf_op jit(solution)/shard_map/all_to_all | solution.py:100
  68.4 0.1 all-gather.3.cloned.1.call-update
  68.5 0.1 reduce-scatter.8.cloned.1.call-start
  68.6 53.7 %all_to_all.36 = bf16[16,64,1024]{2,1,0:T(8,128)(2,1)S(1)} all-to-all(bf16[16,64,1024]{2,1,0:T(8,128)(2,1)S(1)} %bitcast.65), channel_id=1, replica_groups=mesh['grp'=2,'ep'=16,'tp'=8] {'ep'}, dimensions={0} | all-to-all | bytes 4194304 | tf_op jit(solution)/shard_map/all_to_all | solution.py:106
  122.2 0.2 fusion.31
  122.4 0.0 all-gather.5.cloned.1.call-done
  122.4 4.7 %fusion = f32[512,512]{1,0:T(8,128)S(1)} fusion(bf16[512,3072]{1,0:T(8,128)(2,1)} %all-gather.5.cloned.1.call-done, bf16[4096,512]{1,0:T(8,128)(2,1)} %pad_maximum_fusion), kind=kOutput, calls=%fused_computation.1 | convolution fusion | flops 1610612736 | bytes 7340032 | tf_op jit(solution)/shard_map/dot_general | solution.py:18
  127.1 1.9 convolution_add_fusion
  129.0 0.9 fusion.14.hidden
  129.9 7.2 %down.3 = (bf16[8,512,384]{2,1,0:T(8,128)(2,1)}, bf16[512,1024]{1,0:T(8,128)(2,1)}) custom-call(bf16[512,256]{1,0:T(8,128)(2,1)} %fusion.14.hidden, bf16[256,4096]{1,0:T(8,128)(2,1)} %bitcast.92), custom_call_target="tpu_custom_call" | custom-call | flops 1073741824 | bytes 6553600 | tf_op jit(solution)/shard_map/down/pallas_call | solution.py:54
  137.1 0.1 reduce-scatter.8.cloned.1.call-update
  137.1 0.1 reduce-scatter.6.cloned.1.call-start
  137.2 2.5 all-gather.3.cloned.1.call-done
  139.7 4.6 %fusion.2 = f32[512,512]{1,0:T(8,128)S(1)} fusion(bf16[512,3072]{1,0:T(8,128)(2,1)} %all-gather.3.cloned.1.call-done, bf16[4096,512]{1,0:T(8,128)(2,1)} %pad_maximum_fusion), kind=kOutput, calls=%fused_computation.3 | convolution fusion | flops 1610612736 | bytes 7340032 | tf_op jit(solution)/shard_map/dot_general | solution.py:18
  144.3 1.9 convolution_add_fusion.1
  146.2 0.9 fusion.15.hidden
  147.1 7.2 %down.2 = (bf16[8,512,384]{2,1,0:T(8,128)(2,1)}, bf16[512,1024]{1,0:T(8,128)(2,1)}) custom-call(bf16[512,256]{1,0:T(8,128)(2,1)} %fusion.15.hidden, bf16[256,4096]{1,0:T(8,128)(2,1)} %bitcast.93), custom_call_target="tpu_custom_call" | custom-call | flops 1073741824 | bytes 6553600 | tf_op jit(solution)/shard_map/down/pallas_call | solution.py:54
  154.3 0.1 reduce-scatter.6.cloned.1.call-update
  154.4 0.1 reduce-scatter.10.cloned.1.call-start
  154.5 0.0 copy-done.2
  154.5 1.1 copy-done.3
  155.5 0.2 pad_maximum_fusion.1
  155.8 60.6 %all_to_all.37 = bf16[16,64,1024]{2,1,0:T(8,128)(2,1)S(1)} all-to-all(bf16[16,64,1024]{2,1,0:T(8,128)(2,1)S(1)} %pad_maximum_fusion.1), channel_id=1, replica_groups=mesh['grp'=2,'ep'=16,'tp'=8] {'ep'}, dimensions={0} | all-to-all | bytes 4194304 | tf_op jit(solution)/shard_map/all_to_all | solution.py:130
  216.4 0.7 fusion.36
  217.1 0.7 fusion.4
  217.8 1.0 copy.10
  218.9 0.1 reduce-scatter.10.cloned.1.call-update
  218.9 0.0 reduce-scatter.8.cloned.1.call-done
  219.0 3.7 %all-to-all-start.4 = ((bf16[16,32,384]{2,1,0:T(8,128)(2,1)}), bf16[16,32,384]{2,1,0:T(8,128)(2,1)S(1)}, u32[]{:S(2)}, u32[]{:S(2)}) async-start(bf16[16,32,384]{2,1,0:T(8,128)(2,1)} %bitcast.78), calls=%async_computation.6 | async-start | bytes 786432 | tf_op jit(solution)/shard_map/all_to_all | solution.py:137
  222.7 15.4 %reduce-scatter.6.cloned.1.call-done = bf16[1,512,384]{2,1,0:T(8,128)(2,1)} async-done(((bf16[8,512,384]{2,1,0:T(8,128)(2,1)}), bf16[1,512,384]{2,1,0:T(8,128)(2,1)}) %reduce-scatter.6.cloned.1.call-update) | async-done | bytes 393232 | tf_op jit(solution)/shard_map/reduce_scatter | solution.py:128
  238.2 0.0 all-to-all-done.4
  238.2 11.2 %all-to-all-start.3 = ((bf16[16,32,384]{2,1,0:T(8,128)(2,1)}), bf16[16,32,384]{2,1,0:T(8,128)(2,1)S(1)}, u32[]{:S(2)}, u32[]{:S(2)}) async-start(bf16[16,32,384]{2,1,0:T(8,128)(2,1)} %bitcast.79), calls=%async_computation.4 | async-start | bytes 786432 | tf_op jit(solution)/shard_map/all_to_all | solution.py:137
  249.4 28.5 %reduce-scatter.10.cloned.1.call-done = bf16[128,256]{1,0:T(8,128)(2,1)} async-done(((bf16[1024,256]{1,0:T(8,128)(2,1)}), bf16[128,256]{1,0:T(8,128)(2,1)}) %reduce-scatter.10.cloned.1.call-update) | async-done | bytes 65552
  277.8 0.9 copy.11
  278.8 0.1 convert_reduce_fusion
  278.9 0.3 convolution_bitcast_fusion
  279.2 0.3 convolution_bitcast_fusion.1
  279.6 0.0 copy-start.4
  279.6 0.0 copy-start.5
  279.6 0.0 all-to-all-done.3
  279.6 0.3 convolution_bitcast_fusion.2
  279.9 0.4 fusion.35
  280.4 0.1 multiply_reduce_fusion
  280.5 11.1 %all_to_all.38 = f32[8,2,256]{2,1,0:T(2,128)S(1)} all-to-all(f32[8,2,256]{2,1,0:T(2,128)S(1)} %broadcast_in_dim.49), channel_id=1, replica_groups=mesh['grp'=2,'ep'=16,'tp'=8] {'tp'}, dimensions={0} | all-to-all | bytes 32768 | tf_op jit(solution)/shard_map/all_to_all | solution.py:144
  291.7 0.0 copy-done.4
  291.7 0.9 add_convert_fusion
  (15 shorter events, 0.1 us)
Async XLA Ops:
  6.5 29.8 %copy-start.6 = (f32[256,2]{0,1:T(2,128)S(1)}, f32[256,2]{0,1:T(2,128)}, u32[]{:S(2)}) copy-start(f32[256,2]{0,1:T(2,128)} %param.10) | copy-start | bytes 6148
  10.6 38.5 %all-to-all-start = ((bf16[16,32,384]{2,1,0:T(8,128)(2,1)}), bf16[16,32,384]{2,1,0:T(8,128)(2,1)S(1)}, u32[]{:S(2)}, u32[]{:S(2)}) async-start(bf16[16,32,384]{2,1,0:T(8,128)(2,1)} %bitcast.4), calls=%async_computation | async-start | bytes 786432 | tf_op jit(solution)/shard_map/all_to_all | solution.py:100
  34.3 88.1 %all-gather.5.cloned.1.call-start = ((), (), s32[]{:S(2)}) async-start(), calls=%async_computation.11 | async-start | bytes 3538944 | tf_op jit(solution)/shard_map/all_gather | solution.py:110
  34.4 2.3 copy-start
  49.0 0.8 copy-start.1
  49.9 89.8 %all-gather.3.cloned.1.call-start = ((), (), s32[]{:S(2)}) async-start(), calls=%async_computation.10 | async-start | bytes 3538944 | tf_op jit(solution)/shard_map/all_gather | solution.py:110
  68.5 150.5 %reduce-scatter.8.cloned.1.call-start = ((), (), s32[]{:S(2)}) async-start(), calls=%async_computation.13 | async-start | bytes 3538944 | tf_op jit(solution)/shard_map/reduce_scatter | solution.py:128
  137.1 101.0 %reduce-scatter.6.cloned.1.call-start = ((), (), s32[]{:S(2)}) async-start(), calls=%async_computation.12 | async-start | bytes 3538944 | tf_op jit(solution)/shard_map/reduce_scatter | solution.py:128
  147.1 7.4 %copy-start.2 = (bf16[512,1024]{1,0:T(8,128)(2,1)S(1)}, bf16[512,1024]{1,0:T(8,128)(2,1)}, u32[]{:S(2)}) copy-start(bf16[512,1024]{1,0:T(8,128)(2,1)} %get-tuple-element.24) | copy-start | bytes 3145732
  154.3 1.2 copy-start.3
  154.4 123.4 %reduce-scatter.10.cloned.1.call-start = ((), (), s32[]{:S(2)}) async-start(), calls=%async_computation.14 | async-start | bytes 589824
  219.0 19.2 %all-to-all-start.4 = ((bf16[16,32,384]{2,1,0:T(8,128)(2,1)}), bf16[16,32,384]{2,1,0:T(8,128)(2,1)S(1)}, u32[]{:S(2)}, u32[]{:S(2)}) async-start(bf16[16,32,384]{2,1,0:T(8,128)(2,1)} %bitcast.78), calls=%async_computation.6 | async-start | bytes 786432 | tf_op jit(solution)/shard_map/all_to_all | solution.py:137
  238.2 41.4 %all-to-all-start.3 = ((bf16[16,32,384]{2,1,0:T(8,128)(2,1)}), bf16[16,32,384]{2,1,0:T(8,128)(2,1)S(1)}, u32[]{:S(2)}, u32[]{:S(2)}) async-start(bf16[16,32,384]{2,1,0:T(8,128)(2,1)} %bitcast.79), calls=%async_computation.4 | async-start | bytes 786432 | tf_op jit(solution)/shard_map/all_to_all | solution.py:137
  279.6 12.1 %copy-start.4 = (f32[512]{0:T(512)S(1)}, f32[512]{0:T(512)}, u32[]{:S(2)}) copy-start(f32[512]{0:T(512)} %param.15) | copy-start | bytes 6148
  279.6 12.1 %copy-start.5 = (f32[512]{0:T(512)S(1)}, f32[512]{0:T(512)}, u32[]{:S(2)}) copy-start(f32[512]{0:T(512)} %param.14) | copy-start | bytes 6148
Sparse Core Ops, SparseCore 0:
  50.0 42.1 all-gather.4
  94.0 45.5 all-gather.2
  142.2 45.5 reduce-scatter.7
  190.3 47.8 reduce-scatter.5
  240.5 37.2 reduce-scatter.9
